TPU v7x, 32 devices: a whole 2x2x4 slice. The times are simulated.
32 devices in a mesh: grp: 2 (over y), sp: 4 (over z), tp: 4 (over x, core).
Axes of the slice: x: 2, y: 2, z: 4, core: 2. Of those that a mesh axis runs over, the one named last changes fastest.
Arguments:
- stream: bfloat16 [12288, 4096], P(('grp', 'sp', 'tp')), parts along dimension 0, may hold values from -6 to 6
- norm_gain: float32 [2, 4096], replicated, may hold values from 0.1 to 1.9
- mix_weight: bfloat16 [2, 4, 1024, 1024], P(None, None, 'sp', 'tp'), may hold values from -0.1875 to 0.1875
- branch_scale: float32 [2, 4096], replicated, may hold values from 0.1 to 1.9
Outputs:
- result: bfloat16 [12288, 4096], P(('grp', 'sp', 'tp')), parts along dimension 0
There are 2 independent parts, one for each index of `grp`. A program takes and returns all parts, laid end to end along the dimension named above; an argument that names none is the same for every part. Nothing has to cross between parts.
All inputs are finite; a program needn't handle non-finite values.
Results may differ from a plain program's by a relative error of at most 0.0056.
Values may be sent and summed in bfloat16 or wider, within the bound.
A program may use at most 128 MiB of HBM per device.

v0:
```python
import jax
import jax.numpy as jnp
from jax import lax
from jax.sharding import PartitionSpec as P

GW = 1024
G = 4
LAYERS = 2
epsilon = 1e-06
window_lengths = (2, 4, 8, 16)
halo_rows = 15


def from_behind(block, axis, distance):
    devices = range(lax.axis_size(axis))
    route = [(i - distance, i) for i in devices if i - distance in devices]
    return lax.ppermute(block, axis, route)


def per_device(stream, norm_gain, mix_weight, branch_scale):
    row_count = stream.shape[0]
    feature_width = stream.shape[1]
    offset = lax.axis_index(("sp", "tp")) * row_count
    counts_base = (offset + lax.iota(jnp.int32, row_count)).astype(jnp.float32) + 1.0
    residual = stream.astype(jnp.float32)
    for layer_idx in range(LAYERS):
        scale_rows = lax.rsqrt(jnp.mean(residual * residual, axis=1, keepdims=True) + epsilon)
        normed = (residual * scale_rows * norm_gain[layer_idx]).astype(jnp.bfloat16)
        earlier = from_behind(normed[row_count - halo_rows :], ("sp", "tp"), 1)
        extended = jnp.concatenate([earlier, normed], axis=0).astype(jnp.float32)
        pieces = []
        for group_idx in range(G):
            window_len = window_lengths[group_idx]
            segment = extended[:, group_idx * GW : (group_idx + 1) * GW]
            own_rows = segment[halo_rows:]
            running = own_rows
            for back_step in range(1, window_len):
                running = (
                    running + segment[halo_rows - back_step : halo_rows - back_step + row_count]
                )
            window_mean = running / jnp.minimum(counts_base, float(window_len))[:, None]
            pieces.append((window_mean - own_rows).astype(jnp.bfloat16))
        pooled = jnp.stack(pieces, axis=1)
        weight_shard = mix_weight[layer_idx]
        full_rows = lax.all_gather(weight_shard, "sp", axis=1, tiled=True)
        mixed_out = jnp.einsum(
            "rgc,gcn->rgn",
            pooled,
            lax.all_gather(full_rows, "tp", axis=2, tiled=True),
            preferred_element_type=jnp.float32,
        )
        residual = residual + mixed_out.reshape(row_count, feature_width) * branch_scale[layer_idx]
    return residual.astype(jnp.bfloat16)


def solution(mesh):
    return jax.shard_map(
        per_device,
        mesh=mesh,
        in_specs=(P(("grp", "sp", "tp"), None), P(), P(None, None, "sp", "tp"), P()),
        out_specs=P(("grp", "sp", "tp"), None),
        check_vma=False,
    )
```

profile of v0, /device:TPU:9, one launch (start us, length us, event | category | flops | bytes accessed | tf_op | source)
XLA Modules:
  0.0 248.3 jit_solution(16958773101239605890)
XLA Ops:
  6.5 2.2 fusion.69
  8.8 0.0 all-gather.9.cloned.1.call-update
  8.8 0.0 all-gather.13.cloned.1.call-start
  8.9 0.7 all-gather.13.cloned.1.call-update
  9.6 0.0 all-gather.11.cloned.1.call-start
  9.6 44.4 %all-gather.9.cloned.1.call-done = bf16[1,4,1024,256]{3,2,1,0:T(8,128)(2,1)} async-done(((bf16[1,4,256,256]{3,2,1,0:T(8,128)(2,1)}), bf16[1,4,1024,256]{3,2,1,0:T(8,128)(2,1)}) %all-gather.9.cloned.1.call-update) | async-done | bytes 2097168 | tf_op jit(solution)/shard_map/all_gather | solution.py:45
  54.0 0.0 all-gather.11.cloned.1.call-update
  54.0 0.0 all-gather.15.cloned.1.call-start
  54.0 0.7 fusion.4
  54.8 45.3 %all-gather.13.cloned.1.call-done = bf16[1,4,1024,256]{3,2,1,0:T(8,128)(2,1)} async-done(((bf16[1,4,256,256]{3,2,1,0:T(8,128)(2,1)}), bf16[1,4,1024,256]{3,2,1,0:T(8,128)(2,1)}) %all-gather.13.cloned.1.call-update) | async-done | bytes 2097168 | tf_op jit(solution)/shard_map/all_gather | solution.py:45
  100.1 1.0 fusion.6
  101.1 1.7 copy-done.2
  102.8 4.2 %collective-permute-start = (bf16[15,4096]{1,0:T(8,128)(2,1)S(1)}, bf16[15,4096]{1,0:T(8,128)(2,1)S(1)}, u32[]{:S(2)}, u32[]{:S(2)}) collective-permute-start(bf16[15,4096]{1,0:T(8,128)(2,1)S(1)} %slice.340), channel_id=1, source_target_pairs={{0,1},{1,2},{2,3},{3,4},{4,5},{5,6},{6,7},{7,8},{8,9},{9,10},{10,1... | collective-permute-start | bytes 368648 | tf_op jit(solution)/shard_map/ppermute | solution.py:17
  107.1 1.8 collective-permute-done
  108.9 3.2 %maximum_convert_fusion = f32[399,4096]{1,0:T(8,128)S(1)} fusion(bf16[384,4096]{1,0:T(8,128)(2,1)} %copy-done.2, bf16[15,4096]{1,0:T(8,128)(2,1)S(1)} %collective-permute-done), kind=kLoop, calls=%fused_computation.13 | loop fusion | flops 6537216 | bytes 9805824 | tf_op jit(solution)/shard_map/convert_element_type | solution.py:30
  112.2 3.3 %fusion.62 = bf16[384,1,1024]{2,0,1:T(8,128)(2,1)} fusion(f32[384]{0:T(512)S(1)} %fusion.63, f32[399,4096]{1,0:T(8,128)S(1)} %maximum_convert_fusion), kind=kLoop, calls=%fused_computation.114 | loop fusion | flops 7077888 | bytes 25953792 | tf_op jit(solution)/shard_map/stack | solution.py:43
  115.4 3.6 %fusion.56 = (bf16[384,1,1024]{2,0,1:T(8,128)(2,1)}, bf16[384,1,1024]{2,0,1:T(8,128)(2,1)}, bf16[384,1,1024]{2,0,1:T(8,128)(2,1)}) fusion(f32[384]{0:T(512)S(1)} %fusion.66, f32[399,4096]{1,0:T(8,128)S(1)} %maximum_convert_fusion, f32[384]{0:T(512)S(1)} %get-tuple-element.18, f32[384]{0:T(512)S(1)} %get-tuple-element.17), kind=kLoop, calls=%fused_computation.108 | loop fusion | flops 7864320 | bytes 24384000 | tf_op jit(solution)/shard_map/stack | solution.py:43
  119.0 43.0 %all-gather.11.cloned.1.call-done = bf16[1,4,1024,1024]{3,2,1,0:T(8,128)(2,1)} async-done(((bf16[1,4,1024,256]{3,2,1,0:T(8,128)(2,1)}), bf16[1,4,1024,1024]{3,2,1,0:T(8,128)(2,1)}) %all-gather.11.cloned.1.call-update) | async-done | bytes 8388624 | tf_op jit(solution)/shard_map/all_gather | solution.py:49
  162.0 7.8 %fusion.21 = f32[4,48,8,1024]{3,2,1,0:T(8,128)S(1)} fusion(bf16[1,4,1024,1024]{3,2,1,0:T(8,128)(2,1)} %all-gather.11.cloned.1.call-done, bf16[384,1,1024]{2,0,1:T(8,128)(2,1)} %fusion.62, bf16[384,1,1024]{2,0,1:T(8,128)(2,1)} %get-tuple-element.10, bf16[384,1,1024]{2,0,1:T(8,128)(2,1)} %get-tuple-element.9, bf16[384,1,1024]{2,0,1:T(8,128)(2,1)} %get-tuple-element.8), kind=kOutput, calls=%fused_computation.29 | convolution fusion | flops 3225944064 | bytes 17825792 | tf_op jit(solution)/shard_map/rgc,gcn->rgn/dot_general | solution.py:46
  169.8 0.6 copy.7
  170.4 1.2 multiply_reduce_fusion
  171.6 2.0 copy-done
  173.7 1.6 multiply_convert_fusion
  175.3 2.3 collective-permute-start.1
  177.6 4.6 %collective-permute-done.1 = bf16[15,4096]{1,0:T(8,128)(2,1)S(1)} collective-permute-done((bf16[15,4096]{1,0:T(8,128)(2,1)S(1)}, bf16[15,4096]{1,0:T(8,128)(2,1)S(1)}, u32[]{:S(2)}, u32[]{:S(2)}) %collective-permute-start.1) | collective-permute-done | bytes 122912 | tf_op jit(solution)/shard_map/ppermute | solution.py:17
  182.2 0.9 maximum_convert_fusion.1
  183.1 3.3 %fusion.61 = bf16[384,1,1024]{2,0,1:T(8,128)(2,1)} fusion(f32[384]{0:T(512)S(1)} %fusion.63, f32[399,4096]{1,0:T(8,128)S(1)} %maximum_convert_fusion.1), kind=kLoop, calls=%fused_computation.113 | loop fusion | flops 7077888 | bytes 25953792 | tf_op jit(solution)/shard_map/stack | solution.py:43
  186.4 3.5 %fusion.55 = (bf16[384,1,1024]{2,0,1:T(8,128)(2,1)}, bf16[384,1,1024]{2,0,1:T(8,128)(2,1)}, bf16[384,1,1024]{2,0,1:T(8,128)(2,1)}) fusion(f32[384]{0:T(512)S(1)} %fusion.66, f32[399,4096]{1,0:T(8,128)S(1)} %maximum_convert_fusion.1, f32[384]{0:T(512)S(1)} %get-tuple-element.18, f32[384]{0:T(512)S(1)} %get-tuple-element.17), kind=kLoop, calls=%fused_computation.107 | loop fusion | flops 7864320 | bytes 24384000 | tf_op jit(solution)/shard_map/stack | solution.py:43
  189.9 34.3 %all-gather.15.cloned.1.call-done = bf16[1,4,1024,1024]{3,2,1,0:T(8,128)(2,1)} async-done(((bf16[1,4,1024,256]{3,2,1,0:T(8,128)(2,1)}), bf16[1,4,1024,1024]{3,2,1,0:T(8,128)(2,1)}) %all-gather.15.cloned.1.call-update) | async-done | bytes 8388624 | tf_op jit(solution)/shard_map/all_gather | solution.py:49
  224.3 7.9 %fusion.26 = f32[4,48,8,1024]{3,2,1,0:T(8,128)S(1)} fusion(bf16[1,4,1024,1024]{3,2,1,0:T(8,128)(2,1)} %all-gather.15.cloned.1.call-done, bf16[384,1,1024]{2,0,1:T(8,128)(2,1)} %fusion.61, bf16[384,1,1024]{2,0,1:T(8,128)(2,1)} %get-tuple-element.7, bf16[384,1,1024]{2,0,1:T(8,128)(2,1)} %get-tuple-element.6, bf16[384,1,1024]{2,0,1:T(8,128)(2,1)} %get-tuple-element.5), kind=kOutput, calls=%fused_computation.30 | convolution fusion | flops 3225944064 | bytes 17825792 | tf_op jit(solution)/shard_map/rgc,gcn->rgn/dot_general | solution.py:46
  232.2 3.4 %copy.8 = f32[4,48,8,1024]{3,2,0,1:T(8,128)} copy(f32[4,48,8,1024]{3,2,1,0:T(8,128)S(1)} %fusion.26) | data formatting | bytes 12582912 | tf_op jit(solution)/shard_map/reshape | solution.py:52
  235.6 6.2 %add_convert_fusion = bf16[384,4096]{1,0:T(8,128)(2,1)} fusion(f32[384,4096]{1,0:T(8,128)} %bitcast.43, f32[4096]{0:T(1024)S(1)} %bitcast.47, f32[384,4096]{1,0:T(8,128)S(1)} %bitcast.42, f32[4096]{0:T(1024)S(1)} %bitcast.46, bf16[384,4096]{1,0:T(8,128)(2,1)S(1)} %copy-done.1), kind=kLoop, calls=%fused_computation.10 | loop fusion | flops 9437184 | bytes 18907136 | tf_op jit(solution)/shard_map/convert_element_type | solution.py:53
  (24 shorter events, 0.2 us)
Async XLA Ops:
  6.5 47.4 %all-gather.9.cloned.1.call-start = ((), (), s32[]{:S(2)}) async-start(), calls=%async_computation | async-start | bytes 2621440 | tf_op jit(solution)/shard_map/all_gather | solution.py:45
  8.8 45.3 %copy-start.1 = (bf16[384,4096]{1,0:T(8,128)(2,1)S(1)}, bf16[384,4096]{1,0:T(8,128)(2,1)}, u32[]{:S(2)}) copy-start(bf16[384,4096]{1,0:T(8,128)(2,1)} %param.4) | copy-start | bytes 9437188
  8.8 91.2 %all-gather.13.cloned.1.call-start = ((), (), s32[]{:S(2)}) async-start(), calls=%async_computation.2 | async-start | bytes 2621440 | tf_op jit(solution)/shard_map/all_gather | solution.py:45
  9.6 152.5 %all-gather.11.cloned.1.call-start = ((), (), s32[]{:S(2)}) async-start(), calls=%async_computation.1 | async-start | bytes 10485760 | tf_op jit(solution)/shard_map/all_gather | solution.py:49
  54.0 170.3 %all-gather.15.cloned.1.call-start = ((), (), s32[]{:S(2)}) async-start(), calls=%async_computation.3 | async-start | bytes 10485760 | tf_op jit(solution)/shard_map/all_gather | solution.py:49
  54.7 45.3 %copy-start.3 = (f32[2,4096]{1,0:T(2,128)S(1)}, f32[2,4096]{1,0:T(2,128)}, u32[]{:S(2)}) copy-start(f32[2,4096]{1,0:T(2,128)} %param.5) | copy-start | bytes 98308
  100.1 6.9 %copy-start.4 = (f32[2,4096]{1,0:T(2,128)S(1)}, f32[2,4096]{1,0:T(2,128)}, u32[]{:S(2)}) copy-start(f32[2,4096]{1,0:T(2,128)} %param.7) | copy-start | bytes 98308
  101.1 1.7 copy-start.2
  102.8 6.1 %collective-permute-start = (bf16[15,4096]{1,0:T(8,128)(2,1)S(1)}, bf16[15,4096]{1,0:T(8,128)(2,1)S(1)}, u32[]{:S(2)}, u32[]{:S(2)}) collective-permute-start(bf16[15,4096]{1,0:T(8,128)(2,1)S(1)} %slice.340), channel_id=1, source_target_pairs={{0,1},{1,2},{2,3},{3,4},{4,5},{5,6},{6,7},{7,8},{8,9},{9,10},{10,1... | collective-permute-start | bytes 368648 | tf_op jit(solution)/shard_map/ppermute | solution.py:17
  170.4 3.3 %copy-start = (f32[4,48,8,1024]{3,2,0,1:T(8,128)}, f32[4,48,8,1024]{3,2,0,1:T(8,128)S(1)}, u32[]{:S(2)}) copy-start(f32[4,48,8,1024]{3,2,0,1:T(8,128)S(1)} %copy.7) | copy-start | bytes 18874372
  175.3 6.9 %collective-permute-start.1 = (bf16[15,4096]{1,0:T(8,128)(2,1)S(1)}, bf16[15,4096]{1,0:T(8,128)(2,1)S(1)}, u32[]{:S(2)}, u32[]{:S(2)}) collective-permute-start(bf16[15,4096]{1,0:T(8,128)(2,1)S(1)} %slice.371), channel_id=1, source_target_pairs={{0,1},{1,2},{2,3},{3,4},{4,5},{5,6},{6,7},{7,8},{8,9},{9,10},{10,1... | collective-permute-start | bytes 368648 | tf_op jit(solution)/shard_map/ppermute | solution.py:17
  224.3 11.3 %slice-start = ((s8[6291456]{0:T(1024)(128)(4,1)}), s8[4194304]{0:T(1024)(128)(4,1)S(1)}, s32[]{:S(2)}) async-start(s8[6291456]{0:T(1024)(128)(4,1)} %bitcast.40), calls=%async_computation.4 | async-start | bytes 8388608
  224.3 11.3 %slice-start.1 = ((s8[6291456]{0:T(1024)(128)(4,1)}), s8[2097152]{0:T(1024)(128)(4,1)S(1)}, s32[]{:S(2)}) async-start(s8[6291456]{0:T(1024)(128)(4,1)} %bitcast.40), calls=%async_computation.5 | async-start | bytes 4194304
Sparse Core Ops, SparseCore 0:
  8.9 44.9 all-gather.8
  55.5 44.4 all-gather.12
  101.6 60.4 all-gather.10
  163.4 60.7 all-gather.14
where the time goes:
time: 249 us; the launch traced here: 248 us
  waiting for transfers between devices  174 us (70%)
  other arithmetic  28.5 us (11%)
  matrix products  15.6 us (6%)
  between operations  13.3 us (5%)
  local copies, waits for them, and re-layouts  10.1 us (4%)
  starting transfers between devices  6.56 us (3%)
    all_gather x2, waiting for transfers between devices, per_device(): full_rows = lax.all_gather(weight_shard, 'sp', axis=1, tiled=True)  89.6 us
    all_gather x2, waiting for transfers between devices, per_device(): lax.all_gather(full_rows, 'tp', axis=2, tiled=True)  77.3 us
    dot_general x2, matrix products, per_device(): jnp.einsum('rgc,gcn->rgn', pooled, lax.all_gather(full_rows, 'tp', axis=2...  15.6 us
    another operation x4, other arithmetic, per_device(): pooled = jnp.stack(pieces, axis=1)  13.6 us
    ppermute x2, waiting for transfers between devices, from_behind(): return lax.ppermute(block, axis, route)  6.48 us
    ppermute x2, starting transfers between devices, from_behind(): return lax.ppermute(block, axis, route)  6.44 us
    convert_element_type x1, other arithmetic, per_device(): return residual.astype(jnp.bfloat16)  6.2 us
  transfers between devices with their start and end apart: 6, of which 6 were waited for; matrix products, arithmetic and copies ran while one was open for 12% of the time, Pallas kernels for 0%

commit v1 on v0

--- a/solution.py
+++ b/solution.py
@@ -42,7 +42,14 @@
             pieces.append((window_mean - own_rows).astype(jnp.bfloat16))
         pooled = jnp.stack(pieces, axis=1)
         weight_shard = mix_weight[layer_idx]
-        full_rows = lax.all_gather(weight_shard, "sp", axis=1, tiled=True)
+        ring = [weight_shard]
+        for hop in range(3):
+            ring.append(lax.ppermute(ring[-1], "sp", [(dev, (dev + 1) % 4) for dev in range(4)]))
+        full_rows = jnp.roll(
+            jnp.concatenate(ring[::-1], axis=1),
+            (lax.axis_index("sp") + 1) * ring[0].shape[1],
+            axis=1,
+        )
         mixed_out = jnp.einsum(
             "rgc,gcn->rgn",
             pooled,

time: 249 us -> 208 us (0.84)
  waiting for transfers between devices: 174 us -> 97.9 us
  other arithmetic: 28.5 us -> 41.2 us
  matrix products: 15.6 us -> 23.5 us
  starting transfers between devices: 6.56 us -> 14.3 us
  local copies, waits for them, and re-layouts: 10.1 us -> 17.5 us
    all_gather x2 -> x0, waiting for transfers between devices: 89.6 us -> none  [per_device(): full_rows = lax.all_gather(weight_shard, 'sp', axis=1, tiled=True)]
    ppermute x0 -> x6, waiting for transfers between devices: none -> 71.2 us  [per_device(): lax.ppermute(ring[-1], 'sp', [(dev, (dev + 1) % 4) for dev in range(4)])]
    all_gather x2, waiting for transfers between devices: 77.3 us -> 17.6 us  [per_device(): lax.all_gather(full_rows, 'tp', axis=2, tiled=True)]
    reshape x2, local copies, waits for them, and re-layouts: 4.01 us -> 13.4 us  [per_device(): mixed_out.reshape(row_count, feature_width) * branch_scale[layer_idx]]
    concatenate x0 -> x2, other arithmetic: none -> 8.48 us  [per_device(): jnp.roll(jnp.concatenate(ring[::-1], axis=1), (lax.axis_index('sp') + 1)...]
    dot_general x2, matrix products: 15.6 us -> 23.5 us  [per_device(): jnp.einsum('rgc,gcn->rgn', pooled, lax.all_gather(full_rows, 'tp', axis=2...]
    ppermute x2, starting transfers between devices: 6.44 us -> 11.6 us  [from_behind(): return lax.ppermute(block, axis, route)]
    reduce_sum x2, other arithmetic: 1.92 us -> 4.73 us  [per_device(): jnp.mean(residual * residual, axis=1, keepdims=True) + epsilon]
  transfers between devices with their start and end apart: 6 -> 10, of which waited for: 6 -> 9; matrix products, arithmetic and copies ran while one was open for 12% -> 24% of each run, Pallas kernels for 0% -> 0%
where the time goes in v1:
time: 208 us
  waiting for transfers between devices  97.9 us (47%)
  other arithmetic  41.2 us (20%)
  matrix products  23.5 us (11%)
  local copies, waits for them, and re-layouts  17.5 us (8%)
  starting transfers between devices  14.3 us (7%)
  between operations  13.6 us (7%)
    ppermute x6, waiting for transfers between devices, per_device(): lax.ppermute(ring[-1], 'sp', [(dev, (dev + 1) % 4) for dev in range(4)])  71.2 us
    dot_general x2, matrix products, per_device(): jnp.einsum('rgc,gcn->rgn', pooled, lax.all_gather(full_rows, 'tp', axis=2...  23.5 us
    all_gather x2, waiting for transfers between devices, per_device(): lax.all_gather(full_rows, 'tp', axis=2, tiled=True)  17.6 us
    another operation x4, other arithmetic, per_device(): pooled = jnp.stack(pieces, axis=1)  13.7 us
    reshape x2, local copies, waits for them, and re-layouts, per_device(): mixed_out.reshape(row_count, feature_width) * branch_scale[layer_idx]  13.4 us
    ppermute x2, starting transfers between devices, from_behind(): return lax.ppermute(block, axis, route)  11.6 us
    ppermute x2, waiting for transfers between devices, from_behind(): return lax.ppermute(block, axis, route)  9.15 us
    concatenate x2, other arithmetic, per_device(): jnp.roll(jnp.concatenate(ring[::-1], axis=1), (lax.axis_index('sp') + 1)...  8.48 us
  transfers between devices with their start and end apart: 10, of which 9 were waited for; matrix products, arithmetic and copies ran while one was open for 24% of the time, Pallas kernels for 0%

profile of v1, /device:TPU:9, one launch (start us, length us, event | category | flops | bytes accessed | tf_op | source)
XLA Modules:
  0.0 208.0 jit_solution(7850644226723461569)
XLA Ops:
  6.5 1.3 fusion.71
  8.0 1.3 collective-permute-start
  9.4 11.5 %collective-permute-done = bf16[4,256,256]{1,2,0:T(8,128)(2,1)S(1)} collective-permute-done((bf16[4,256,256]{1,2,0:T(8,128)(2,1)S(1)}, bf16[4,256,256]{1,2,0:T(8,128)(2,1)S(1)}, u32[]{:S(2)}, u32[]{:S(2)}) %collective-permute-start) | collective-permute-done | bytes 524320 | tf_op jit(solution)/shard_map/ppermute | solution.py:47
  20.9 1.3 collective-permute-start.1
  22.2 12.1 %collective-permute-done.1 = bf16[4,256,256]{1,2,0:T(8,128)(2,1)S(1)} collective-permute-done((bf16[4,256,256]{1,2,0:T(8,128)(2,1)S(1)}, bf16[4,256,256]{1,2,0:T(8,128)(2,1)S(1)}, u32[]{:S(2)}, u32[]{:S(2)}) %collective-permute-start.1) | collective-permute-done | bytes 524320 | tf_op jit(solution)/shard_map/ppermute | solution.py:47
  34.2 13.2 %collective-permute-done.2 = bf16[4,256,256]{1,2,0:T(8,128)(2,1)S(1)} collective-permute-done((bf16[4,256,256]{1,2,0:T(8,128)(2,1)S(1)}, bf16[4,256,256]{1,2,0:T(8,128)(2,1)S(1)}, u32[]{:S(2)}, u32[]{:S(2)}) %collective-permute-start.2) | collective-permute-done | bytes 524320 | tf_op jit(solution)/shard_map/ppermute | solution.py:47
  47.4 3.6 %fusion.29 = bf16[4,1024,256]{1,2,0:T(8,128)(2,1)} fusion(s32[]{:T(128)S(6)} %select_n.13, bf16[4,256,256]{1,2,0:T(8,128)(2,1)S(1)} %collective-permute-done.2, bf16[4,256,256]{1,2,0:T(8,128)(2,1)S(1)} %collective-permute-done.1, bf16[4,256,256]{1,2,0:T(8,128)(2,1)S(1)} %collective-permute-done, bf16[4,256,256]{1,2,0:T(8,128)(2,1)S(1)} %bitcast.33), kind=kLoop, calls=%fused_computation.53 | loop fusion | flops 16777216 | bytes 4194308 | tf_op jit(solution)/shard_map/jit(_roll_dynamic)/concatenate | solution.py:48
  51.4 12.3 %collective-permute-done.4 = bf16[4,256,256]{1,2,0:T(8,128)(2,1)S(1)} collective-permute-done((bf16[4,256,256]{1,2,0:T(8,128)(2,1)S(1)}, bf16[4,256,256]{1,2,0:T(8,128)(2,1)S(1)}, u32[]{:S(2)}, u32[]{:S(2)}) %collective-permute-start.4) | collective-permute-done | bytes 524320 | tf_op jit(solution)/shard_map/ppermute | solution.py:47
  63.7 11.6 %collective-permute-done.5 = bf16[4,256,256]{1,2,0:T(8,128)(2,1)S(1)} collective-permute-done((bf16[4,256,256]{1,2,0:T(8,128)(2,1)S(1)}, bf16[4,256,256]{1,2,0:T(8,128)(2,1)S(1)}, u32[]{:S(2)}, u32[]{:S(2)}) %collective-permute-start.5) | collective-permute-done | bytes 524320 | tf_op jit(solution)/shard_map/ppermute | solution.py:47
  75.3 10.6 %collective-permute-done.6 = bf16[4,256,256]{1,2,0:T(8,128)(2,1)S(1)} collective-permute-done((bf16[4,256,256]{1,2,0:T(8,128)(2,1)S(1)}, bf16[4,256,256]{1,2,0:T(8,128)(2,1)S(1)}, u32[]{:S(2)}, u32[]{:S(2)}) %collective-permute-start.6) | collective-permute-done | bytes 524320 | tf_op jit(solution)/shard_map/ppermute | solution.py:47
  85.9 4.8 %fusion.22 = bf16[4,1024,256]{1,2,0:T(8,128)(2,1)} fusion(s32[]{:T(128)S(6)} %select_n.13, bf16[4,256,256]{1,2,0:T(8,128)(2,1)S(1)} %collective-permute-done.6, bf16[4,256,256]{1,2,0:T(8,128)(2,1)S(1)} %collective-permute-done.5, bf16[4,256,256]{1,2,0:T(8,128)(2,1)S(1)} %collective-permute-done.4, bf16[4,256,256]{1,2,0:T(8,128)(2,1)} %bitcast.35), kind=kLoop, calls=%fused_computation.46 | loop fusion | flops 16777216 | bytes 4194308 | tf_op jit(solution)/shard_map/jit(_roll_dynamic)/concatenate | solution.py:48
  90.8 0.7 fusion
  91.5 1.0 fusion.2
  92.5 1.7 copy-done.2
  94.2 7.2 %collective-permute-start.3 = (bf16[15,4096]{1,0:T(8,128)(2,1)S(1)}, bf16[15,4096]{1,0:T(8,128)(2,1)S(1)}, u32[]{:S(2)}, u32[]{:S(2)}) collective-permute-start(bf16[15,4096]{1,0:T(8,128)(2,1)S(1)} %slice.340), channel_id=1, source_target_pairs={{0,1},{1,2},{2,3},{3,4},{4,5},{5,6},{6,7},{7,8},{8,9},{9,10},{10,1... | collective-permute-start | bytes 368648 | tf_op jit(solution)/shard_map/ppermute | solution.py:17
  101.5 4.5 %collective-permute-done.3 = bf16[15,4096]{1,0:T(8,128)(2,1)S(1)} collective-permute-done((bf16[15,4096]{1,0:T(8,128)(2,1)S(1)}, bf16[15,4096]{1,0:T(8,128)(2,1)S(1)}, u32[]{:S(2)}, u32[]{:S(2)}) %collective-permute-start.3) | collective-permute-done | bytes 122912 | tf_op jit(solution)/shard_map/ppermute | solution.py:17
  106.1 2.8 %maximum_convert_fusion = f32[399,4096]{1,0:T(8,128)S(1)} fusion(bf16[384,4096]{1,0:T(8,128)(2,1)} %copy-done.2, bf16[15,4096]{1,0:T(8,128)(2,1)S(1)} %collective-permute-done.3), kind=kLoop, calls=%fused_computation.25 | loop fusion | flops 6537216 | bytes 9805824 | tf_op jit(solution)/shard_map/convert_element_type | solution.py:30
  108.9 3.3 %fusion.64 = bf16[384,1,1024]{2,0,1:T(8,128)(2,1)} fusion(f32[384]{0:T(512)S(1)} %fusion.65, f32[399,4096]{1,0:T(8,128)S(1)} %maximum_convert_fusion), kind=kLoop, calls=%fused_computation.140 | loop fusion | flops 7077888 | bytes 25953792 | tf_op jit(solution)/shard_map/stack | solution.py:43
  112.2 3.5 %fusion.58 = (bf16[384,1,1024]{2,0,1:T(8,128)(2,1)}, bf16[384,1,1024]{2,0,1:T(8,128)(2,1)}, bf16[384,1,1024]{2,0,1:T(8,128)(2,1)}) fusion(f32[384]{0:T(512)S(1)} %fusion.68, f32[399,4096]{1,0:T(8,128)S(1)} %maximum_convert_fusion, f32[384]{0:T(512)S(1)} %get-tuple-element.19, f32[384]{0:T(512)S(1)} %get-tuple-element.18), kind=kLoop, calls=%fused_computation.134 | loop fusion | flops 7864320 | bytes 24384000 | tf_op jit(solution)/shard_map/stack | solution.py:43
  115.7 12.2 %fusion.3 = f32[4,1024,384]{2,1,0:T(8,128)} fusion(bf16[4,1024,1024]{1,2,0:T(8,128)(2,1)} %all-gather.3.cloned.1.call-done, bf16[384,1,1024]{2,0,1:T(8,128)(2,1)} %fusion.64, bf16[384,1,1024]{2,0,1:T(8,128)(2,1)} %get-tuple-element.11, bf16[384,1,1024]{2,0,1:T(8,128)(2,1)} %get-tuple-element.10, bf16[384,1,1024]{2,0,1:T(8,128)(2,1)} %get-tuple-element.9), kind=kOutput, calls=%fused_computation.27 | convolution fusion | flops 3225944064 | bytes 17825792 | tf_op jit(solution)/shard_map/rgc,gcn->rgn/dot_general | solution.py:53
  128.0 6.8 %copy.9 = f32[384,4096]{1,0:T(8,128)} copy(f32[384,4096]{0,1:T(8,128)} %bitcast.30) | data formatting | bytes 12582912 | tf_op jit(solution)/shard_map/reshape | solution.py:59
  134.8 4.0 %multiply_reduce_fusion = f32[384]{0:T(512)S(1)} fusion(f32[384,4096]{1,0:T(8,128)} %copy.9, f32[4096]{0:T(1024)S(1)} %bitcast.36, bf16[384,4096]{1,0:T(8,128)(2,1)S(1)} %copy-done.1), kind=kLoop, calls=%fused_computation.8 | loop fusion | flops 7863936 | bytes 9455104 | tf_op jit(solution)/shard_map/reduce_sum | solution.py:27
  139.5 1.6 multiply_convert_fusion
  141.1 4.3 %collective-permute-start.7 = (bf16[15,4096]{1,0:T(8,128)(2,1)S(1)}, bf16[15,4096]{1,0:T(8,128)(2,1)S(1)}, u32[]{:S(2)}, u32[]{:S(2)}) collective-permute-start(bf16[15,4096]{1,0:T(8,128)(2,1)S(1)} %slice.371), channel_id=1, source_target_pairs={{0,1},{1,2},{2,3},{3,4},{4,5},{5,6},{6,7},{7,8},{8,9},{9,10},{10,1... | collective-permute-start | bytes 368648 | tf_op jit(solution)/shard_map/ppermute | solution.py:17
  145.4 4.6 %collective-permute-done.7 = bf16[15,4096]{1,0:T(8,128)(2,1)S(1)} collective-permute-done((bf16[15,4096]{1,0:T(8,128)(2,1)S(1)}, bf16[15,4096]{1,0:T(8,128)(2,1)S(1)}, u32[]{:S(2)}, u32[]{:S(2)}) %collective-permute-start.7) | collective-permute-done | bytes 122912 | tf_op jit(solution)/shard_map/ppermute | solution.py:17
  150.0 0.9 maximum_convert_fusion.1
  150.9 3.3 %fusion.63 = bf16[384,1,1024]{2,0,1:T(8,128)(2,1)} fusion(f32[384]{0:T(512)S(1)} %fusion.65, f32[399,4096]{1,0:T(8,128)S(1)} %maximum_convert_fusion.1), kind=kLoop, calls=%fused_computation.139 | loop fusion | flops 7077888 | bytes 25953792 | tf_op jit(solution)/shard_map/stack | solution.py:43
  154.2 3.6 %fusion.57 = (bf16[384,1,1024]{2,0,1:T(8,128)(2,1)}, bf16[384,1,1024]{2,0,1:T(8,128)(2,1)}, bf16[384,1,1024]{2,0,1:T(8,128)(2,1)}) fusion(f32[384]{0:T(512)S(1)} %fusion.68, f32[399,4096]{1,0:T(8,128)S(1)} %maximum_convert_fusion.1, f32[384]{0:T(512)S(1)} %get-tuple-element.19, f32[384]{0:T(512)S(1)} %get-tuple-element.18), kind=kLoop, calls=%fused_computation.133 | loop fusion | flops 7864320 | bytes 24384000 | tf_op jit(solution)/shard_map/stack | solution.py:43
  157.8 17.6 %all-gather.5.cloned.1.call-done = bf16[4,1024,1024]{1,2,0:T(8,128)(2,1)} async-done(((bf16[4,1024,256]{1,2,0:T(8,128)(2,1)}), bf16[4,1024,1024]{1,2,0:T(8,128)(2,1)}) %all-gather.5.cloned.1.call-update) | async-done | bytes 8388624 | tf_op jit(solution)/shard_map/all_gather | solution.py:56
  175.4 11.3 %fusion.11 = f32[4,1024,384]{2,1,0:T(8,128)} fusion(bf16[4,1024,1024]{1,2,0:T(8,128)(2,1)} %all-gather.5.cloned.1.call-done, bf16[384,1,1024]{2,0,1:T(8,128)(2,1)} %fusion.63, bf16[384,1,1024]{2,0,1:T(8,128)(2,1)} %get-tuple-element.8, bf16[384,1,1024]{2,0,1:T(8,128)(2,1)} %get-tuple-element.7, bf16[384,1,1024]{2,0,1:T(8,128)(2,1)} %get-tuple-element.6), kind=kOutput, calls=%fused_computation.35 | convolution fusion | flops 3225944064 | bytes 17825792 | tf_op jit(solution)/shard_map/rgc,gcn->rgn/dot_general | solution.py:53
  186.6 6.5 %copy.10 = f32[384,4096]{1,0:T(8,128)} copy(f32[384,4096]{0,1:T(8,128)} %bitcast.31) | data formatting | bytes 12582912 | tf_op jit(solution)/shard_map/reshape | solution.py:59
  193.2 8.0 %add_convert_fusion = bf16[384,4096]{1,0:T(8,128)(2,1)} fusion(f32[384,4096]{1,0:T(8,128)} %copy.10, f32[4096]{0:T(1024)S(1)} %bitcast.40, f32[384,4096]{1,0:T(8,128)} %copy.9, f32[4096]{0:T(1024)S(1)} %bitcast.38, bf16[384,4096]{1,0:T(8,128)(2,1)S(1)} %copy-done.1), kind=kLoop, calls=%fused_computation.6 | loop fusion | flops 9437184 | bytes 18907136 | tf_op jit(solution)/shard_map/convert_element_type | solution.py:60
  (31 shorter events, 1.3 us)
Async XLA Ops:
  6.5 109.2 %all-gather.3.cloned.1.call-start = ((), (), s32[]{:S(2)}) async-start(), calls=%async_computation | async-start | bytes 10485760 | tf_op jit(solution)/shard_map/all_gather | solution.py:56
  8.0 12.9 %collective-permute-start = (bf16[4,256,256]{1,2,0:T(8,128)(2,1)S(1)}, bf16[4,256,256]{1,2,0:T(8,128)(2,1)S(1)}, u32[]{:S(2)}, u32[]{:S(2)}) collective-permute-start(bf16[4,256,256]{1,2,0:T(8,128)(2,1)S(1)} %bitcast.32), channel_id=1, source_target_pairs={{0,4},{4,8},{8,12},{12,0},{1,5},{5,9},{9,13},{13,1},{2,6},{6,10},{... | collective-permute-start | bytes 1572872 | tf_op jit(solution)/shard_map/ppermute | solution.py:47
  20.9 13.4 %collective-permute-start.1 = (bf16[4,256,256]{1,2,0:T(8,128)(2,1)S(1)}, bf16[4,256,256]{1,2,0:T(8,128)(2,1)S(1)}, u32[]{:S(2)}, u32[]{:S(2)}) collective-permute-start(bf16[4,256,256]{1,2,0:T(8,128)(2,1)S(1)} %collective-permute-done), channel_id=1, source_target_pairs={{0,4},{4,8},{8,12},{12,0},{1,5},{5,9},{9,13},{13,1},{2,6},{6,10},{... | collective-permute-start | bytes 1572872 | tf_op jit(solution)/shard_map/ppermute | solution.py:47
  34.2 13.2 %collective-permute-start.2 = (bf16[4,256,256]{1,2,0:T(8,128)(2,1)S(1)}, bf16[4,256,256]{1,2,0:T(8,128)(2,1)S(1)}, u32[]{:S(2)}, u32[]{:S(2)}) collective-permute-start(bf16[4,256,256]{1,2,0:T(8,128)(2,1)S(1)} %collective-permute-done.1), channel_id=1, source_target_pairs={{0,4},{4,8},{8,12},{12,0},{1,5},{5,9},{9,13},{13,1},{2,6},{6,10},{... | collective-permute-start | bytes 1572872 | tf_op jit(solution)/shard_map/ppermute | solution.py:47
  51.0 24.2 %copy-start.4 = (f32[2,4096]{1,0:T(2,128)S(1)}, f32[2,4096]{1,0:T(2,128)}, u32[]{:S(2)}) copy-start(f32[2,4096]{1,0:T(2,128)} %param.7) | copy-start | bytes 98308
  51.1 124.3 %all-gather.5.cloned.1.call-start = ((), (), s32[]{:S(2)}) async-start(), calls=%async_computation.1 | async-start | bytes 10485760 | tf_op jit(solution)/shard_map/all_gather | solution.py:56
  51.3 24.0 %copy-start.3 = (bf16[1,4,256,256]{2,3,1,0:T(8,128)(2,1)}, bf16[1,4,256,256]{2,3,1,0:T(8,128)(2,1)S(1)}, u32[]{:S(2)}) copy-start(bf16[1,4,256,256]{2,3,1,0:T(8,128)(2,1)S(1)} %copy.12) | copy-start | bytes 1572868
  51.3 12.4 %collective-permute-start.4 = (bf16[4,256,256]{1,2,0:T(8,128)(2,1)S(1)}, bf16[4,256,256]{1,2,0:T(8,128)(2,1)S(1)}, u32[]{:S(2)}, u32[]{:S(2)}) collective-permute-start(bf16[4,256,256]{1,2,0:T(8,128)(2,1)S(1)} %bitcast.34), channel_id=1, source_target_pairs={{0,4},{4,8},{8,12},{12,0},{1,5},{5,9},{9,13},{13,1},{2,6},{6,10},{... | collective-permute-start | bytes 1572872 | tf_op jit(solution)/shard_map/ppermute | solution.py:47
  63.7 11.6 %collective-permute-start.5 = (bf16[4,256,256]{1,2,0:T(8,128)(2,1)S(1)}, bf16[4,256,256]{1,2,0:T(8,128)(2,1)S(1)}, u32[]{:S(2)}, u32[]{:S(2)}) collective-permute-start(bf16[4,256,256]{1,2,0:T(8,128)(2,1)S(1)} %collective-permute-done.4), channel_id=1, source_target_pairs={{0,4},{4,8},{8,12},{12,0},{1,5},{5,9},{9,13},{13,1},{2,6},{6,10},{... | collective-permute-start | bytes 1572872 | tf_op jit(solution)/shard_map/ppermute | solution.py:47
  75.3 10.6 %collective-permute-start.6 = (bf16[4,256,256]{1,2,0:T(8,128)(2,1)S(1)}, bf16[4,256,256]{1,2,0:T(8,128)(2,1)S(1)}, u32[]{:S(2)}, u32[]{:S(2)}) collective-permute-start(bf16[4,256,256]{1,2,0:T(8,128)(2,1)S(1)} %collective-permute-done.5), channel_id=1, source_target_pairs={{0,4},{4,8},{8,12},{12,0},{1,5},{5,9},{9,13},{13,1},{2,6},{6,10},{... | collective-permute-start | bytes 1572872 | tf_op jit(solution)/shard_map/ppermute | solution.py:47
  85.9 4.9 %copy-start.1 = (bf16[384,4096]{1,0:T(8,128)(2,1)S(1)}, bf16[384,4096]{1,0:T(8,128)(2,1)}, u32[]{:S(2)}) copy-start(bf16[384,4096]{1,0:T(8,128)(2,1)} %param.6) | copy-start | bytes 9437188
  91.5 10.0 %copy-start.5 = (f32[2,4096]{1,0:T(2,128)S(1)}, f32[2,4096]{1,0:T(2,128)}, u32[]{:S(2)}) copy-start(f32[2,4096]{1,0:T(2,128)} %param.9) | copy-start | bytes 98308
  92.5 1.7 copy-start.2
  94.2 11.9 %collective-permute-start.3 = (bf16[15,4096]{1,0:T(8,128)(2,1)S(1)}, bf16[15,4096]{1,0:T(8,128)(2,1)S(1)}, u32[]{:S(2)}, u32[]{:S(2)}) collective-permute-start(bf16[15,4096]{1,0:T(8,128)(2,1)S(1)} %slice.340), channel_id=1, source_target_pairs={{0,1},{1,2},{2,3},{3,4},{4,5},{5,6},{6,7},{7,8},{8,9},{9,10},{10,1... | collective-permute-start | bytes 368648 | tf_op jit(solution)/shard_map/ppermute | solution.py:17
  134.8 4.7 %copy-start = (f32[384,4096]{1,0:T(8,128)S(1)}, f32[384,4096]{1,0:T(8,128)}, u32[]{:S(2)}) copy-start(f32[384,4096]{1,0:T(8,128)} %copy.9) | copy-start | bytes 18874372
  141.1 8.9 %collective-permute-start.7 = (bf16[15,4096]{1,0:T(8,128)(2,1)S(1)}, bf16[15,4096]{1,0:T(8,128)(2,1)S(1)}, u32[]{:S(2)}, u32[]{:S(2)}) collective-permute-start(bf16[15,4096]{1,0:T(8,128)(2,1)S(1)} %slice.371), channel_id=1, source_target_pairs={{0,1},{1,2},{2,3},{3,4},{4,5},{5,6},{6,7},{7,8},{8,9},{9,10},{10,1... | collective-permute-start | bytes 368648 | tf_op jit(solution)/shard_map/ppermute | solution.py:17
Sparse Core Ops, SparseCore 0:
  51.2 62.8 all-gather.2
  115.7 59.6 all-gather.4
